TPU v7x, 32 devices: a whole 2x2x4 slice. The times are simulated.
32 devices in a mesh: ep: 8 (over z, x), tp: 4 (over y, core).
Axes of the slice: x: 2, y: 2, z: 4, core: 2. Of those that a mesh axis runs over, the one named last changes fastest.
Arguments:
- queries: bfloat16 [1024, 4096], P('ep', 'tp'), may hold values from -6 to 6
- key_rows: bfloat16 [1024, 4096], P('ep', 'tp'), may hold values from -6 to 6
- value_rows: bfloat16 [1024, 4096], P('ep', 'tp'), may hold values from -6 to 6
- key_shift: bfloat16 [1024, 64], P('ep', 'tp'), may hold values from -20 to 1
- out_weight: bfloat16 [4096, 4096], P('tp'), may hold values from -0.09375 to 0.09375
- routed_rows: bfloat16 [1024, 4096], P('ep'), may hold values from -6 to 6
- expert_ids: int32 [1024, 2], P('ep'), may hold values from 0 to 7, as said below
- route_weights: float32 [1024, 2], P(('ep', 'tp')), may hold values from 0.2 to 1
- gate_weight: bfloat16 [8, 4096, 1024], P('ep', None, 'tp'), may hold values from -0.09375 to 0.09375
- up_weight: bfloat16 [8, 4096, 1024], P('ep', None, 'tp'), may hold values from -0.09375 to 0.09375
- down_weight: bfloat16 [8, 1024, 4096], P('ep', 'tp'), may hold values from -0.1875 to 0.1875
Outputs:
- mixed_rows: bfloat16 [1024, 4096], P(('ep', 'tp'))
- routed_out: bfloat16 [1024, 4096], P(('ep', 'tp'))
Inputs may be any that keep to these rules, and one draw needn't show every extreme that they name: `expert_ids`: the two ids of a token differ and lie in one group of 2 consecutive experts. Within each aligned block of 32 tokens no expert is named more than 16 times.
All inputs are finite; a program needn't handle non-finite values.
Results may differ from a plain program's by a relative error of at most 0.015.
Values may be sent and summed in bfloat16 or wider, within the bound.
A program may use at most 128 MiB of HBM per device.

v0:
```python
import jax
import jax.numpy as jnp
from jax import lax
from jax.sharding import PartitionSpec as P

HEAD = 64
KEY_BLOCK = 512


def stick_attend(query_rows, key_all, value_all, shift_all, first_pos):
    row_count = query_rows.shape[0]
    head_count = query_rows.shape[1]
    head_depth = query_rows.shape[2]
    query_pos = first_pos + jnp.arange(row_count, dtype=jnp.int32)
    last_block = (first_pos + row_count - 1) // KEY_BLOCK
    score_scale = head_depth ** (-0.5)

    def sweep_block(step_index, state_pair):
        running, logsum = state_pair
        row_start = (last_block - step_index) * KEY_BLOCK
        key_tile_block = lax.dynamic_slice_in_dim(key_all, row_start, KEY_BLOCK, 0).reshape(
            KEY_BLOCK, head_count, head_depth
        )
        value_block = lax.dynamic_slice_in_dim(value_all, row_start, KEY_BLOCK, 0).reshape(
            KEY_BLOCK, head_count, head_depth
        )
        shift_block = lax.dynamic_slice_in_dim(shift_all, row_start, KEY_BLOCK, 0).astype(
            jnp.float32
        )
        scores = (
            jnp.einsum(
                "thd,shd->hts", query_rows, key_tile_block, preferred_element_type=jnp.float32
            )
            * score_scale
        )
        scores = scores + shift_block.T[:, None, :]
        key_pos = row_start + jnp.arange(KEY_BLOCK, dtype=jnp.int32)
        strict = (key_pos[None, :] < query_pos[:, None])[None]
        log_keep = jnp.where(strict, jax.nn.log_sigmoid(-scores), 0.0)
        suffix = lax.cumsum(log_keep, axis=2, reverse=True) - log_keep + logsum[:, :, None]
        weight = jnp.where(strict, jnp.exp(jax.nn.log_sigmoid(scores) + suffix), 0.0).astype(
            jnp.bfloat16
        )
        running = running + jnp.einsum(
            "hts,shd->htd", weight, value_block, preferred_element_type=jnp.float32
        )
        return (running, logsum + jnp.sum(log_keep, axis=2))

    initial = (
        jnp.zeros((head_count, row_count, head_depth), jnp.float32),
        jnp.zeros((head_count, row_count), jnp.float32),
    )
    running, logsum = lax.fori_loop(0, last_block + 1, sweep_block, initial)
    return (
        jnp.transpose(running, (1, 0, 2))
        .reshape(row_count, head_count * head_depth)
        .astype(jnp.bfloat16)
    )


def slot_numbers(pair_ids, expert_count):
    one_hot = (pair_ids[..., None] == jnp.arange(expert_count, dtype=jnp.int32)).astype(jnp.int32)
    earlier = jnp.cumsum(one_hot, axis=1) - one_hot
    return jnp.sum(one_hot * earlier, axis=2)


def pack_rows(source_rows, destination, slot_count):
    pair_count = destination.shape[0]
    matches = destination[None, :] == jnp.arange(slot_count, dtype=jnp.int32)[:, None]
    source_index = jnp.sum(
        jnp.where(matches, jnp.arange(pair_count, dtype=jnp.int32)[None, :] // 2, 0), axis=1
    )
    filled = jnp.any(matches, axis=1)
    picked = jnp.take(source_rows, source_index, axis=0)
    return jnp.where(filled[:, None], picked, jnp.zeros_like(picked))


def expand(expert_rows, gate_part, up_part):
    gate_proj = jnp.einsum(
        "rcd,df->rcf", expert_rows, gate_part, preferred_element_type=jnp.float32
    )
    up_proj = jnp.einsum("rcd,df->rcf", expert_rows, up_part, preferred_element_type=jnp.float32)
    return (jax.nn.silu(gate_proj) * up_proj).astype(jnp.bfloat16)


def shards(
    queries,
    key_rows,
    value_rows,
    key_shift,
    out_weight,
    routed_rows,
    expert_ids,
    route_weights,
    gate_weight,
    up_weight,
    down_weight,
):
    tp_count = lax.axis_size("tp")
    local_rows = queries.shape[0]
    heads_here = key_shift.shape[1]
    key_all, value_all, shift_all = (
        lax.all_gather(key_rows, "ep", axis=0, tiled=True),
        lax.all_gather(value_rows, "ep", axis=0, tiled=True),
        lax.all_gather(key_shift, "ep", axis=0, tiled=True),
    )
    first_pos = lax.axis_index("ep") * local_rows
    attended = stick_attend(
        queries.reshape(local_rows, heads_here, HEAD), key_all, value_all, shift_all, first_pos
    )
    mixed_rows = lax.psum_scatter(
        jnp.dot(attended, out_weight, preferred_element_type=jnp.float32).astype(jnp.bfloat16),
        "tp",
        scatter_dimension=0,
        tiled=True,
    )
    expert_count = lax.axis_size("ep")
    sub_rows = local_rows // tp_count
    capacity = 4 * sub_rows // expert_count
    model_width = routed_rows.shape[1]
    column = lax.axis_index("tp")
    own_ids = lax.dynamic_slice_in_dim(expert_ids, column * sub_rows, sub_rows, 0).reshape(
        1, sub_rows * 2
    )
    own_slot = slot_numbers(own_ids, expert_count)[0]
    own_dest = own_ids[0] * capacity + own_slot
    own_input = lax.dynamic_slice_in_dim(routed_rows, column * sub_rows, sub_rows, 0)
    outgoing = pack_rows(own_input, own_dest, expert_count * capacity).reshape(
        expert_count, capacity, model_width
    )
    arrived = lax.all_to_all(outgoing, "ep", split_axis=0, concat_axis=0, tiled=True)
    hidden = expand(lax.all_gather(arrived, "tp", axis=1, tiled=True), gate_weight[0], up_weight[0])
    unit_count = hidden.shape[2]
    ordered = jnp.transpose(
        hidden.reshape(expert_count, tp_count, capacity, unit_count), (1, 0, 2, 3)
    )
    ordered = ordered.reshape(tp_count * expert_count * capacity, unit_count)
    partial_value = lax.psum_scatter(
        jnp.dot(ordered, down_weight[0], preferred_element_type=jnp.float32).astype(jnp.bfloat16),
        "tp",
        scatter_dimension=0,
        tiled=True,
    )
    returned = lax.all_to_all(
        partial_value.reshape(expert_count, capacity, model_width),
        "ep",
        split_axis=0,
        concat_axis=0,
        tiled=True,
    )
    picked = jnp.take(returned.reshape(expert_count * capacity, model_width), own_dest, axis=0)
    picked = picked.reshape(sub_rows, 2, model_width).astype(jnp.float32)
    routed_out = (
        picked[:, 0] * route_weights[:, 0:1] + picked[:, 1] * route_weights[:, 1:2]
    ).astype(jnp.bfloat16)
    return (mixed_rows, routed_out)


def solution(mesh):
    return jax.shard_map(
        shards,
        mesh=mesh,
        in_specs=(
            P("ep", "tp"),
            P("ep", "tp"),
            P("ep", "tp"),
            P("ep", "tp"),
            P("tp", None),
            P("ep", None),
            P("ep", None),
            P(("ep", "tp"), None),
            P("ep", None, "tp"),
            P("ep", None, "tp"),
            P("ep", "tp", None),
        ),
        out_specs=(P(("ep", "tp"), None), P(("ep", "tp"), None)),
        check_vma=False,
    )
```

profile of v0, /device:TPU:0, one launch (start us, length us, event | category | flops | bytes accessed | tf_op | source)
XLA Modules:
  0.0 289.4 jit_solution(12918340799919668226)
XLA Ops:
  8.1 0.9 broadcast_multiply_fusion
  9.8 1.0 constant_dynamic-slice_fusion.2
  10.9 1.2 gather_fusion
  12.3 32.9 %all_to_all.10 = bf16[8,16,4096]{2,1,0:T(8,128)(2,1)} all-to-all(bf16[8,16,4096]{2,1,0:T(8,128)(2,1)S(1)} %select_select_fusion), channel_id=1, replica_groups=mesh['ep'=8,'tp'=4] {'ep'}, dimensions={0} | all-to-all | bytes 2097152 | tf_op jit(solution)/shard_map/all_to_all | solution.py:131
  45.3 33.6 %all-gather.8.cloned.1.call-done = bf16[8,64,4096]{2,1,0:T(8,128)(2,1)} async-done(((bf16[8,16,4096]{2,1,0:T(8,128)(2,1)}), bf16[8,64,4096]{2,1,0:T(8,128)(2,1)}) %all-gather.8.cloned.1.call-update) | async-done | bytes 4194320 | tf_op jit(solution)/shard_map/all_gather | solution.py:132
  79.0 4.2 %fusion.21 = f32[8,64,256]{2,1,0:T(8,128)S(1)} fusion(bf16[8,64,4096]{2,1,0:T(8,128)(2,1)} %all-gather.8.cloned.1.call-done, bf16[1,4096,256]{2,1,0:T(8,128)(2,1)} %param.21), kind=kOutput, calls=%fused_computation.40 | convolution fusion | flops 1073741824 | bytes 6815744 | tf_op jit(solution)/shard_map/rcd,df->rcf/dot_general | solution.py:79
  83.7 1.2 fusion.26
  85.0 3.2 %convolution_convert_fusion = bf16[512,4096]{1,0:T(8,128)(2,1)} fusion(bf16[512,256]{1,0:T(8,128)(2,1)S(1)} %bitcast.130, bf16[1,256,4096]{2,1,0:T(8,128)(2,1)S(1)} %copy-done), kind=kOutput, calls=%fused_computation.35 | convolution fusion | flops 1075838976 | bytes 6553600 | tf_op jit(solution)/shard_map/dot_general | solution.py:139
  90.5 26.2 %all_gather.13 = bf16[1024,16]{0,1:T(8,128)(2,1)S(1)} all-gather(bf16[128,16]{0,1:T(8,128)(2,1)S(1)} %copy-done.6), channel_id=1, replica_groups=mesh['ep'=8,'tp'=4] {'ep'}, dimensions={0}, use_global_device_ids=true | all-gather | bytes 36864 | tf_op jit(solution)/shard_map/all_gather | solution.py:105
  116.7 16.3 %reduce-scatter.5.cloned.1.call-done = bf16[128,4096]{1,0:T(8,128)(2,1)} async-done(((bf16[512,4096]{1,0:T(8,128)(2,1)}), bf16[128,4096]{1,0:T(8,128)(2,1)}) %reduce-scatter.5.cloned.1.call-update) | async-done | bytes 1048592 | tf_op jit(solution)/shard_map/reduce_scatter | solution.py:138
  133.0 5.5 %all-to-all-start.1 = ((bf16[8,16,4096]{2,1,0:T(8,128)(2,1)}), bf16[8,16,4096]{2,1,0:T(8,128)(2,1)S(1)}, u32[]{:S(2)}, u32[]{:S(2)}) async-start(bf16[8,16,4096]{2,1,0:T(8,128)(2,1)} %bitcast.131), calls=%async_computation.3 | async-start | bytes 2097152 | tf_op jit(solution)/shard_map/all_to_all | solution.py:144
  138.5 3.4 %all-gather.4.cloned.1.call-done = bf16[1024,1024]{0,1:T(8,128)(2,1)} async-done(((bf16[128,1024]{0,1:T(8,128)(2,1)}), bf16[1024,1024]{0,1:T(8,128)(2,1)}) %all-gather.4.cloned.1.call-update) | async-done | bytes 2097168 | tf_op jit(solution)/shard_map/all_gather | solution.py:103
  142.0 57.7 %all-gather.6.cloned.1.call-done = bf16[1024,1024]{0,1:T(8,128)(2,1)} async-done(((bf16[128,1024]{0,1:T(8,128)(2,1)}), bf16[1024,1024]{0,1:T(8,128)(2,1)}) %all-gather.6.cloned.1.call-update) | async-done | bytes 2097168 | tf_op jit(solution)/shard_map/all_gather | solution.py:104
  200.5 25.9 %while.13 = (s32[]{:T(128)}, f32[16,128,64]{1,2,0:T(8,128)}, f32[16,128]{1,0:T(8,128)S(1)}, s32[]{:T(128)}, s32[]{:T(128)}, /*index=5*/bf16[1024,1024]{0,1:T(8,1...) while((s32[]{:T(128)}, f32[16,128,64]{1,2,0:T(8,128)}, ...), condition=%wide.region_4.5_spmd.clone, body=%wide.region_0.4_spmd.clone.sunk | while | flops 438540928 | bytes 58463500 | solution.py:53
  200.5 1.7 constant_dynamic-slice_fusion.6
  202.4 4.0 %fusion.61 = (f32[16,128]{1,0:T(8,128)S(1)}, f32[16,128,512]{1,2,0:T(8,128)S(1)}, f32[16,512,128]{2,1,0:T(8,128)S(1)}) fusion(f32[16,512]{1,0:T(8,128)S(1)} %convert_bitcast_fusion.2, pred[128,512]{0,1:T(8,128)(4,1)S(1)} %broadcast_compare_fusion.2, bf16[512,16,64]{0,2,1:T(8,128)(2,1)S(1)} %bitcast.126, bf16[128,16,64]{0,2,1:T(8,128)(2,1)S(1)} %get-tuple-element.217), kind=kOutput, calls=%fused_computation.34.clone.1 | convolution fusion | flops 145750016 | bytes 9805824 | tf_op jit(solution)/shard_map/while/body/thd,shd->hts/dot_general | solution.py:31
  206.4 10.1 %fusion.62 = f32[16,128,4,128]{1,0,3,2:T(8,128)S(1)} fusion(f32[16,128,4,128]{1,3,2,0:T(8,128)S(1)} %bitcast.124), kind=kOutput, calls=%fused_computation.21.clone.1 | output fusion | flops 133169152 | bytes 8388608 | tf_op jit(solution)/shard_map/reduce-window
  216.8 1.4 copy.62
  218.2 6.8 %fusion.64 = bf16[16,128,512]{1,2,0:T(8,128)(2,1)S(1)} fusion(f32[16,128,4,128]{1,3,2,0:T(8,128)S(1)} %copy.62, f32[16,512,128]{2,1,0:T(8,128)S(1)} %get-tuple-element.181, f32[16,128]{1,0:T(8,128)S(1)} %get-tuple-element.199, f32[16,512]{1,0:T(8,128)S(1)} %convert_bitcast_fusion.2, pred[128,512]{0,1:T(8,128)(4,1)S(1)} %broadcast_compare_fusion.2), kind=kLoop, calls=%fused_computation.9.clone.1 | loop fusion | flops 24117248 | bytes 10592256 | tf_op jit(solution)/shard_map/while/body/convert_element_type | solution.py:41
  226.5 1.1 convert_element_type.43
  227.5 5.6 %convolution_convert_fusion.1 = bf16[128,4096]{1,0:T(8,128)(2,1)} fusion(bf16[128,1024]{0,1:T(8,128)(2,1)S(1)} %bitcast.129, bf16[1024,4096]{1,0:T(8,128)(2,1)} %param.17), kind=kOutput, calls=%fused_computation.36 | convolution fusion | flops 1074266112 | bytes 9699328 | tf_op jit(solution)/shard_map/dot_general | solution.py:112
  233.4 1.7 gather_fusion.1
  235.1 1.4 gather.15
  238.0 44.3 %reduce-scatter.3.cloned.1.call-done = bf16[32,4096]{1,0:T(8,128)(2,1)} async-done(((bf16[128,4096]{1,0:T(8,128)(2,1)}), bf16[32,4096]{1,0:T(8,128)(2,1)}) %reduce-scatter.3.cloned.1.call-update) | async-done | bytes 262160 | tf_op jit(solution)/shard_map/reduce_scatter | solution.py:111
  (70 shorter events, 8.4 us)
Async XLA Ops:
  8.0 77.0 %copy-start = (bf16[1,256,4096]{2,1,0:T(8,128)(2,1)S(1)}, bf16[1,256,4096]{2,1,0:T(8,128)(2,1)}, u32[]{:S(2)}) copy-start(bf16[1,256,4096]{2,1,0:T(8,128)(2,1)} %param.23) | copy-start | bytes 6291460
  8.0 70.9 %all-gather.8.cloned.1.call-start = ((), (), s32[]{:S(2)}) async-start(), calls=%async_computation.7 | async-start | bytes 5242880 | tf_op jit(solution)/shard_map/all_gather | solution.py:132
  45.3 87.7 %reduce-scatter.5.cloned.1.call-start = ((), (), s32[]{:S(2)}) async-start(), calls=%async_computation.8 | async-start | bytes 5242880 | tf_op jit(solution)/shard_map/reduce_scatter | solution.py:138
  79.0 4.3 %copy-start.8 = (bf16[8,64,4096]{2,1,0:T(8,128)(2,1)S(1)}, bf16[8,64,4096]{2,1,0:T(8,128)(2,1)}, u32[]{:S(2)}) copy-start(bf16[8,64,4096]{2,1,0:T(8,128)(2,1)} %all-gather.8.cloned.1.call-done) | copy-start | bytes 12582916
  79.0 4.7 %copy-start.9 = (bf16[1,4096,256]{2,1,0:T(8,128)(2,1)S(1)}, bf16[1,4096,256]{2,1,0:T(8,128)(2,1)}, u32[]{:S(2)}) copy-start(bf16[1,4096,256]{2,1,0:T(8,128)(2,1)} %param.22) | copy-start | bytes 6291460
  85.0 3.3 %copy-start.3 = (bf16[128,1024]{1,0:T(8,128)(2,1)S(1)}, bf16[128,1024]{1,0:T(8,128)(2,1)}, u32[]{:S(2)}) copy-start(bf16[128,1024]{1,0:T(8,128)(2,1)} %param.14) | copy-start | bytes 786436
  85.0 4.2 %copy-start.4 = (bf16[128,1024]{1,0:T(8,128)(2,1)S(1)}, bf16[128,1024]{1,0:T(8,128)(2,1)}, u32[]{:S(2)}) copy-start(bf16[128,1024]{1,0:T(8,128)(2,1)} %param.15) | copy-start | bytes 786436
  88.2 1.9 copy-start.5
  88.2 2.3 copy-start.6
  88.2 28.5 %copy-start.7 = (f32[32,2]{0,1:T(2,128)S(1)}, f32[32,2]{0,1:T(2,128)}, u32[]{:S(2)}) copy-start(f32[32,2]{0,1:T(2,128)} %param.20) | copy-start | bytes 772
  88.2 53.7 %all-gather.4.cloned.1.call-start = ((), (), s32[]{:S(2)}) async-start(), calls=%async_computation.4 | async-start | bytes 2359296 | tf_op jit(solution)/shard_map/all_gather | solution.py:103
  89.2 110.5 %all-gather.6.cloned.1.call-start = ((), (), s32[]{:S(2)}) async-start(), calls=%async_computation.5 | async-start | bytes 2359296 | tf_op jit(solution)/shard_map/all_gather | solution.py:104
  133.0 100.5 %all-to-all-start.1 = ((bf16[8,16,4096]{2,1,0:T(8,128)(2,1)}), bf16[8,16,4096]{2,1,0:T(8,128)(2,1)S(1)}, u32[]{:S(2)}, u32[]{:S(2)}) async-start(bf16[8,16,4096]{2,1,0:T(8,128)(2,1)} %bitcast.131), calls=%async_computation.3 | async-start | bytes 2097152 | tf_op jit(solution)/shard_map/all_to_all | solution.py:144
  138.5 143.8 %reduce-scatter.3.cloned.1.call-start = ((), (), s32[]{:S(2)}) async-start(), calls=%async_computation.6 | async-start | bytes 1310720 | tf_op jit(solution)/shard_map/reduce_scatter | solution.py:111
  218.2 6.8 %copy-start.1 = (f32[16,128,64]{1,2,0:T(8,128)S(1)}, f32[16,128,64]{1,2,0:T(8,128)}, u32[]{:S(2)}) copy-start(f32[16,128,64]{1,2,0:T(8,128)} %get-tuple-element.198) | copy-start | bytes 1572868 | tf_op jit(solution)/shard_map/while
  225.7 0.8 copy-start.2
Sparse Core Ops, SparseCore 0:
  45.4 33.4 all-gather.7
  88.4 44.5 reduce-scatter.4
  233.3 48.8 reduce-scatter.2
Sparse Core Ops, SparseCore 1:
  91.3 50.6 all-gather.3
  144.5 55.2 all-gather.5
where the time goes:
time: 290 us; the launch traced here: 289 us
  waiting for transfers between devices  155 us (53%)
  blocking collectives  59.1 us (20%)
  other arithmetic  21.6 us (7%)
  matrix products  19 us (7%)
  between operations  15.4 us (5%)
  local copies, waits for them, and re-layouts  13 us (4%)
  starting transfers between devices  5.71 us (2%)
    all_gather x1, waiting for transfers between devices, shards(): lax.all_gather(value_rows, 'ep', axis=0, tiled=True)  57.7 us
    reduce_scatter x1, waiting for transfers between devices, shards(): lax.psum_scatter(jnp.dot(attended, out_weight, preferred_element_type=jnp...  44.3 us
    all_gather x1, waiting for transfers between devices, shards(): lax.all_gather(arrived, 'tp', axis=1, tiled=True)  33.6 us
    all_to_all x1, blocking collectives, shards(): lax.all_to_all(outgoing, 'ep', split_axis=0, concat_axis=0, tiled=True)  32.9 us
    all_gather x1, blocking collectives, shards(): lax.all_gather(key_shift, 'ep', axis=0, tiled=True)  26.2 us
    reduce_scatter x1, waiting for transfers between devices, shards(): lax.psum_scatter(jnp.dot(ordered, down_weight[0], preferred_element_type=...  16.3 us
    another operation x2, other arithmetic  10.1 us
    convert_element_type x1, other arithmetic, sweep_block(): jnp.where(strict, jnp.exp(jax.nn.log_sigmoid(scores) + suffix), 0.0)  6.78 us
  transfers between devices with their start and end apart: 6, of which 5 were waited for; matrix products, arithmetic and copies ran while one was open for 14% of the time, Pallas kernels for 0%

commit v1 on v0

--- a/solution.py
+++ b/solution.py
@@ -1,10 +1,15 @@
 import jax
 import jax.numpy as jnp
 from jax import lax
+from jax.experimental import pallas as pl
+from jax.experimental.pallas import tpu as pltpu
 from jax.sharding import PartitionSpec as P
 
 HEAD = 64
 KEY_BLOCK = 512
+GROUPS = 4
+TILE = 256
+MESH = pl.DeviceIdType.MESH
 
 
 def stick_attend(query_rows, key_all, value_all, shift_all, first_pos):
@@ -81,6 +86,507 @@
     )
     up_proj = jnp.einsum("rcd,df->rcf", expert_rows, up_part, preferred_element_type=jnp.float32)
     return (jax.nn.silu(gate_proj) * up_proj).astype(jnp.bfloat16)
+
+
+def meet(devices):
+    barrier = pltpu.get_barrier_semaphore()
+    for ep_to, tp_to in devices:
+        pl.semaphore_signal(
+            barrier, inc=1, device_id={"ep": ep_to, "tp": tp_to}, device_id_type=MESH
+        )
+    pl.semaphore_wait(barrier, len(devices))
+
+
+def push(src, dst, send, recv, ep_to, tp_to):
+    copy = pltpu.make_async_remote_copy(
+        src_ref=src,
+        dst_ref=dst,
+        send_sem=send,
+        recv_sem=recv,
+        device_id={"ep": ep_to, "tp": tp_to},
+        device_id_type=MESH,
+    )
+    copy.start()
+    return copy
+
+
+def spread_kernel(
+    ep_count, q_ref, k_ref, v_ref, s_ref, rows_ref, qkv_ref, shift_ref, gath_ref,
+    send_a, recv_a, send_b, recv_b, own_sem, block_sem,
+):
+    e = lax.axis_index("ep")
+    t = lax.axis_index("tp")
+    g = e // 2
+    x = e % 2
+    e_x = g * 2 + (1 - x)
+    t_y = (t + 2) % 4
+    t_c = t + 1 - 2 * (t % 2)
+    t_yc = (t_c + 2) % 4
+    block = q_ref.shape[0]
+    width = q_ref.shape[1] // ep_count
+    peers = [((e + d) % ep_count, t) for d in range(1, ep_count)]
+    meet(peers + [(e, t_y), (e, t_c)])
+
+    sends = []
+
+    def forward(z, xi, ti, ep_to, tp_to):
+        place = gath_ref.at[z, xi, ti]
+        sends.append(
+            push(place, place, send_b.at[len(sends)], recv_b.at[z, xi, ti], ep_to, tp_to)
+        )
+
+    def arrived(z, xi, ti):
+        place = gath_ref.at[z, xi, ti]
+        pltpu.make_async_copy(place, place, recv_b.at[z, xi, ti]).wait()
+
+    for dz in (3, 2, 1):
+        to = (g + dz) % GROUPS
+        sends.append(
+            push(
+                rows_ref.at[to],
+                gath_ref.at[g, x, t],
+                send_b.at[len(sends)],
+                recv_b.at[g, x, t],
+                to * 2 + x,
+                t,
+            )
+        )
+    for ep_to, tp_to in ((e_x, t), (e, t_y), (e, t_c)):
+        sends.append(
+            push(
+                rows_ref.at[g],
+                gath_ref.at[g, x, t],
+                send_b.at[len(sends)],
+                recv_b.at[g, x, t],
+                ep_to,
+                tp_to,
+            )
+        )
+    keep = pltpu.make_async_copy(rows_ref.at[g], gath_ref.at[g, x, t], block_sem)
+    keep.start()
+    exchange = []
+    owns = []
+    mine = pl.ds(pl.multiple_of(e * width, width), width)
+    here = pl.ds(pl.multiple_of(e * block, block), block)
+    for i, ref in enumerate((q_ref, k_ref, v_ref)):
+        own = pltpu.make_async_copy(ref.at[:, mine], qkv_ref.at[i, here], own_sem.at[i])
+        own.start()
+        owns.append(own)
+    own = pltpu.make_async_copy(s_ref.at[e], shift_ref.at[e], own_sem.at[3])
+    own.start()
+    owns.append(own)
+    for d in range(1, ep_count):
+        to = (e + d) % ep_count
+        cols = pl.ds(pl.multiple_of(to * width, width), width)
+        for i, ref in enumerate((q_ref, k_ref, v_ref)):
+            exchange.append(
+                push(
+                    ref.at[:, cols],
+                    qkv_ref.at[i, here],
+                    send_a.at[i, d - 1],
+                    recv_a.at[i, d - 1],
+                    to,
+                    t,
+                )
+            )
+        exchange.append(
+            push(
+                s_ref.at[to], shift_ref.at[e], send_a.at[3, d - 1], recv_a.at[3, d - 1], to, t
+            )
+        )
+    order = (0, 3, 1, 2)
+    for dz in order[1:]:
+        z = (g + dz) % GROUPS
+        arrived(z, x, t)
+        forward(z, x, t, e_x, t)
+        forward(z, x, t, e, t_y)
+        forward(z, x, t, e, t_c)
+    for dz in order:
+        z = (g + dz) % GROUPS
+        arrived(z, 1 - x, t)
+        if dz in (0, 3):
+            forward(z, 1 - x, t, e, t_y)
+        forward(z, 1 - x, t, e, t_c)
+        arrived(z, x, t_y)
+        if dz not in (0, 3):
+            forward(z, x, t_y, e_x, t)
+        forward(z, x, t_y, e, t_c)
+    for dz in order:
+        z = (g + dz) % GROUPS
+        arrived(z, 1 - x, t_y)
+        forward(z, 1 - x, t_y, e, t_c)
+    for dz in order:
+        z = (g + dz) % GROUPS
+        for xi in (x, 1 - x):
+            arrived(z, xi, t_c)
+            arrived(z, xi, t_yc)
+    for copy in exchange:
+        copy.wait()
+    for copy in sends:
+        copy.wait_send()
+    keep.wait()
+    for copy in owns:
+        copy.wait()
+
+
+def spread(q, k, v, shift_rows, rows, ep_count, tp_count):
+    block = q.shape[0]
+    width = q.shape[1] // ep_count
+    slots, row_width = rows.shape[1:]
+    any_spec = pl.BlockSpec(memory_space=pl.ANY)
+    vmem_spec = pl.BlockSpec(memory_space=pltpu.VMEM)
+
+    def kernel(*refs):
+        spread_kernel(ep_count, *refs)
+
+    return pl.pallas_call(
+        kernel,
+        out_shape=(
+            jax.ShapeDtypeStruct((3, block * ep_count, width), jnp.bfloat16),
+            jax.ShapeDtypeStruct(shift_rows.shape, jnp.float32),
+            jax.ShapeDtypeStruct((GROUPS, 2, tp_count, slots, row_width), jnp.bfloat16),
+        ),
+        in_specs=[vmem_spec] * 5,
+        out_specs=(any_spec,) * 3,
+        scratch_shapes=[
+            pltpu.SemaphoreType.DMA((4, ep_count - 1)),
+            pltpu.SemaphoreType.DMA((4, ep_count - 1)),
+            pltpu.SemaphoreType.DMA((31,)),
+            pltpu.SemaphoreType.DMA((GROUPS, 2, tp_count)),
+            pltpu.SemaphoreType.DMA((4,)),
+            pltpu.SemaphoreType.DMA,
+        ],
+        compiler_params=pltpu.CompilerParams(collective_id=0, has_side_effects=True),
+    )(q, k, v, shift_rows, rows)
+
+
+def stick_kernel(qkv_ref, shift_ref, tri_ref, out_ref):
+    total = qkv_ref.shape[1]
+    width = qkv_ref.shape[2]
+    heads = width // HEAD
+    per = shift_ref.shape[2]
+    scale = HEAD ** (-0.5)
+    lane = lax.broadcasted_iota(jnp.int32, (TILE, width), 1) // HEAD
+    strict = lax.broadcasted_iota(jnp.int32, (TILE, TILE), 1) < lax.broadcasted_iota(
+        jnp.int32, (TILE, TILE), 0
+    )
+    tri = tri_ref[...]
+    for i in range(total // TILE):
+        q_all = qkv_ref[0, i * TILE : (i + 1) * TILE]
+        result = jnp.zeros((TILE, width), jnp.float32)
+        q_heads = [jnp.where(lane == h, q_all, jnp.zeros_like(q_all)) for h in range(heads)]
+        running = [jnp.zeros((TILE, width), jnp.float32) for _ in range(heads)]
+        logsum = [jnp.zeros((TILE, 1), jnp.float32) for _ in range(heads)]
+        for j in range(i, -1, -1):
+            k_all = qkv_ref[1, j * TILE : (j + 1) * TILE]
+            v_all = qkv_ref[2, j * TILE : (j + 1) * TILE]
+            for h in range(heads):
+                shift = jnp.concatenate(
+                    [
+                        shift_ref[j * (TILE // per) + p, h : h + 1]
+                        for p in range(TILE // per)
+                    ],
+                    axis=1,
+                )
+                score = (
+                    lax.dot_general(
+                        q_heads[h],
+                        k_all,
+                        (((1,), (1,)), ((), ())),
+                        preferred_element_type=jnp.float32,
+                    )
+                    * scale
+                    + shift
+                )
+                tail = jnp.log(1.0 + jnp.exp(-jnp.abs(score)))
+                log_take = jnp.minimum(score, 0.0) - tail
+                log_keep = -jnp.maximum(score, 0.0) - tail
+                if i == j:
+                    log_keep = jnp.where(strict, log_keep, 0.0)
+                high = log_keep.astype(jnp.bfloat16)
+                low = (log_keep - high.astype(jnp.float32)).astype(jnp.bfloat16)
+                later = jnp.dot(high, tri, preferred_element_type=jnp.float32) + jnp.dot(
+                    low, tri, preferred_element_type=jnp.float32
+                )
+                weight = jnp.exp(log_take + later + logsum[h])
+                if i == j:
+                    weight = jnp.where(strict, weight, 0.0)
+                running[h] = running[h] + jnp.dot(
+                    weight.astype(jnp.bfloat16), v_all, preferred_element_type=jnp.float32
+                )
+                logsum[h] = logsum[h] + later[:, :1] + log_keep[:, :1]
+        for h in range(heads):
+            result = jnp.where(lane == h, running[h], result)
+        out_ref[i * TILE : (i + 1) * TILE] = result.astype(jnp.bfloat16)
+
+
+def stick(qkv, shift_rows):
+    position = jnp.arange(TILE, dtype=jnp.int32)
+    tri = (position[:, None] > position[None, :]).astype(jnp.bfloat16)
+    vmem_spec = pl.BlockSpec(memory_space=pltpu.VMEM)
+    return pl.pallas_call(
+        stick_kernel,
+        out_shape=jax.ShapeDtypeStruct(qkv.shape[1:], jnp.bfloat16),
+        in_specs=[vmem_spec] * 3,
+        out_specs=vmem_spec,
+    )(qkv, shift_rows, tri)
+
+
+def regroup_kernel(ep_count, att_ref, out_ref, send, recv, own_sem):
+    e = lax.axis_index("ep")
+    t = lax.axis_index("tp")
+    block = out_ref.shape[0]
+    width = att_ref.shape[1]
+    meet([((e + d) % ep_count, t) for d in range(1, ep_count)])
+    cols = pl.ds(pl.multiple_of(e * width, width), width)
+    copies = []
+    for d in range(1, ep_count):
+        to = (e + d) % ep_count
+        part = pl.ds(pl.multiple_of(to * block, block), block)
+        copies.append(
+            push(att_ref.at[part], out_ref.at[:, cols], send.at[d - 1], recv.at[d - 1], to, t)
+        )
+    own = pltpu.make_async_copy(
+        att_ref.at[pl.ds(pl.multiple_of(e * block, block), block)], out_ref.at[:, cols], own_sem
+    )
+    own.start()
+    for copy in copies:
+        copy.wait()
+    own.wait()
+
+
+def regroup(attended, ep_count):
+    rows, width = attended.shape
+
+    def kernel(*refs):
+        regroup_kernel(ep_count, *refs)
+
+    return pl.pallas_call(
+        kernel,
+        out_shape=jax.ShapeDtypeStruct((rows // ep_count, width * ep_count), jnp.bfloat16),
+        in_specs=[pl.BlockSpec(memory_space=pltpu.VMEM)],
+        out_specs=pl.BlockSpec(memory_space=pl.ANY),
+        scratch_shapes=[
+            pltpu.SemaphoreType.DMA((ep_count - 1,)),
+            pltpu.SemaphoreType.DMA((ep_count - 1,)),
+            pltpu.SemaphoreType.DMA,
+        ],
+        compiler_params=pltpu.CompilerParams(collective_id=1, has_side_effects=True),
+    )(attended)
+
+
+def collect_kernel(
+    part_ref, proj_ref, mixed_ref, home_ref,
+    got_c, got_o, pair, pair_o, got_x, got_y, mid_x, mid_y, got_x2, got_y2, got_oy, final,
+    send, recv, recv_z,
+):
+    e = lax.axis_index("ep")
+    t = lax.axis_index("tp")
+    g = e // 2
+    x = e % 2
+    y = t // 2
+    c = t % 2
+    e_x = g * 2 + (1 - x)
+    t_y = (t + 2) % 4
+    t_c = t + 1 - 2 * c
+    others = [((g + dz) % GROUPS * 2 + x, t) for dz in range(1, GROUPS)]
+    meet(others + [(e_x, t), (e, t_y), (e, t_c)])
+    half = GROUPS // 2
+    copies = []
+
+    def go(src, dst, ep_to, tp_to):
+        n = len(copies)
+        copy = push(src, dst, send.at[n], recv.at[n], ep_to, tp_to)
+        copies.append(copy)
+        return copy
+
+    def add(a, b):
+        return (a.astype(jnp.float32) + b.astype(jnp.float32)).astype(jnp.bfloat16)
+
+    swaps = {}
+    firsts = []
+    for zi in range(half):
+        for k in range(2):
+            firsts.append(("x", zi, k))
+            firsts.append(("y", zi, k))
+    seconds = []
+    for zi in range(half):
+        for k in range(2):
+            seconds.append(("x2", zi, k))
+            seconds.append(("y2", zi, k))
+
+    def spot(kind, zi, k):
+        if kind == "x":
+            return zi, 1 - x, k
+        if kind == "y":
+            return half + zi, k, 1 - y
+        if kind == "x2":
+            return zi, x, k
+        return half + zi, k, y
+
+    swap_o = [None, None]
+    for item in firsts + seconds:
+        z, xi, yi = spot(*item)
+        swaps[item] = go(
+            part_ref.at[z, xi, yi * 2 + 1 - c], got_c.at[z, xi, yi], e, t_c
+        )
+        if item == firsts[-1]:
+            for k in range(2):
+                yk = 1 - y if k == 0 else y
+                swap_o[k] = go(proj_ref.at[yk * 2 + 1 - c], got_o.at[yk], e, t_c)
+    hops = {}
+    for item in firsts:
+        kind, zi, k = item
+        z, xi, yi = spot(*item)
+        swaps[item].wait_recv()
+        pair[z, xi, yi] = add(part_ref[z, xi, yi * 2 + c], got_c[z, xi, yi])
+        if kind == "x":
+            hops[item] = go(pair.at[z, xi, yi], got_x.at[zi, k], e_x, t)
+        else:
+            hops[item] = go(pair.at[z, xi, yi], got_y.at[zi, k], e, t_y)
+    swap_o[0].wait_recv()
+    pair_o[1 - y] = add(proj_ref[(1 - y) * 2 + c], got_o[1 - y])
+    hop_o = go(pair_o.at[1 - y], got_oy, e, t_y)
+    for item in seconds:
+        z, xi, yi = spot(*item)
+        swaps[item].wait_recv()
+        pair[z, xi, yi] = add(part_ref[z, xi, yi * 2 + c], got_c[z, xi, yi])
+    swap_o[1].wait_recv()
+    pair_o[y] = add(proj_ref[y * 2 + c], got_o[y])
+    last = []
+    for zi in range(half):
+        for k in range(2):
+            hops[("x", zi, k)].wait_recv()
+            mid_x[zi, k] = add(pair[zi, x, k], got_x[zi, k])
+            hops[("y", zi, k)].wait_recv()
+            mid_y[zi, k] = add(pair[half + zi, k, y], got_y[zi, k])
+        last.append(
+            (
+                go(mid_x.at[zi, 1 - y], got_x2.at[zi], e, t_y),
+                go(mid_y.at[zi, 1 - x], got_y2.at[zi], e_x, t),
+            )
+        )
+    hop_o.wait_recv()
+    mixed_ref[...] = add(pair_o[y], got_oy[...])
+    for zi in range(half):
+        last[zi][0].wait_recv()
+        final[zi] = add(mid_x[zi, y], got_x2[zi])
+        last[zi][1].wait_recv()
+        final[half + zi] = add(mid_y[zi, x], got_y2[zi])
+    backs = []
+    for dz in range(1, GROUPS):
+        to = (g + dz) % GROUPS
+        copy = push(
+            final.at[to], home_ref.at[g], send.at[len(copies) + dz - 1], recv_z.at[dz - 1],
+            to * 2 + x, t,
+        )
+        backs.append(copy)
+    home_ref[g] = final[g]
+    for copy in copies:
+        copy.wait_send()
+    for copy in backs:
+        copy.wait()
+
+
+def collect(part, proj):
+    _, _, tp_count, slots, model_width = part.shape
+    sub = proj.shape[1]
+    half = GROUPS // 2
+    vmem_spec = pl.BlockSpec(memory_space=pltpu.VMEM)
+    bf = jnp.bfloat16
+    block = (slots, model_width)
+    return pl.pallas_call(
+        collect_kernel,
+        out_shape=(
+            jax.ShapeDtypeStruct((sub, model_width), bf),
+            jax.ShapeDtypeStruct((GROUPS, *block), bf),
+        ),
+        in_specs=[vmem_spec] * 2,
+        out_specs=(vmem_spec,) * 2,
+        scratch_shapes=[
+            pltpu.VMEM((GROUPS, 2, 2, *block), bf),
+            pltpu.VMEM((2, sub, model_width), bf),
+            pltpu.VMEM((GROUPS, 2, 2, *block), bf),
+            pltpu.VMEM((2, sub, model_width), bf),
+            pltpu.VMEM((half, 2, *block), bf),
+            pltpu.VMEM((half, 2, *block), bf),
+            pltpu.VMEM((half, 2, *block), bf),
+            pltpu.VMEM((half, 2, *block), bf),
+            pltpu.VMEM((half, *block), bf),
+            pltpu.VMEM((half, *block), bf),
+            pltpu.VMEM((sub, model_width), bf),
+            pltpu.VMEM((GROUPS, *block), bf),
+            pltpu.SemaphoreType.DMA((40,)),
+            pltpu.SemaphoreType.DMA((40,)),
+            pltpu.SemaphoreType.DMA((GROUPS - 1,)),
+        ],
+        compiler_params=pltpu.CompilerParams(
+            collective_id=2, has_side_effects=True, vmem_limit_bytes=60000 * 1024
+        ),
+    )(part, proj)
+
+
+def shards_paired(
+    queries, key_rows, value_rows, key_shift, out_weight, routed_rows, expert_ids,
+    route_weights, gate_weight, up_weight, down_weight,
+):
+    ep_count = lax.axis_size("ep")
+    tp_count = lax.axis_size("tp")
+    local_rows = queries.shape[0]
+    sub = local_rows // tp_count
+    slots = 4 * sub // ep_count
+    model_width = routed_rows.shape[1]
+    column = lax.axis_index("tp")
+    x = lax.axis_index("ep") % 2
+
+    ids = lax.dynamic_slice_in_dim(expert_ids, column * sub, sub, 0)
+    own_rows = lax.dynamic_slice_in_dim(routed_rows, column * sub, sub, 0)
+    group = ids[:, 0] // 2
+    token = jnp.arange(sub, dtype=jnp.int32)
+    earlier = (group[:, None] == group[None, :]) & (token[None, :] < token[:, None])
+    place = group * slots + jnp.sum(earlier.astype(jnp.int32), axis=1)
+    pick = place[None, :] == jnp.arange(GROUPS * slots, dtype=jnp.int32)[:, None]
+    packed = jnp.dot(pick.astype(jnp.bfloat16), own_rows, preferred_element_type=jnp.float32)
+    side = [
+        jnp.sum(jnp.where(ids % 2 == s, route_weights, 0.0), axis=1) for s in range(2)
+    ]
+    pieces = []
+    for weights in side:
+        spread_w = jnp.sum(jnp.where(pick, weights[None, :], 0.0), axis=1)
+        first = lax.reduce_precision(spread_w, 8, 7)
+        second = lax.reduce_precision(spread_w - first, 8, 7)
+        pieces += [first, second, spread_w - first - second]
+    extra = jnp.pad(jnp.stack(pieces, axis=1), ((0, 0), (0, 128 - len(pieces))))
+    rows = jnp.concatenate([packed.astype(jnp.bfloat16), extra.astype(jnp.bfloat16)], axis=1)
+    rows = rows.reshape(GROUPS, slots, model_width + 128)
+
+    per = key_shift.shape[1] // ep_count
+    shift_rows = key_shift.astype(jnp.float32).T.reshape(ep_count, per, local_rows)
+    shift_rows = jnp.pad(shift_rows, ((0, 0), (0, -per % 8), (0, 0)))
+    qkv, shift_all, gathered = spread(
+        queries, key_rows, value_rows, shift_rows, rows, ep_count, tp_count
+    )
+    attended = regroup(stick(qkv, shift_all), ep_count)
+    proj = jnp.dot(attended, out_weight, preferred_element_type=jnp.float32).astype(jnp.bfloat16)
+
+    gathered = gathered.reshape(-1, model_width + 128)
+    expert_rows = gathered[:, :model_width]
+    marks = lax.dynamic_slice_in_dim(gathered[:, model_width:], 3 * x, 3, 1).astype(jnp.float32)
+    scale = marks[:, 0:1] + marks[:, 1:2] + marks[:, 2:3]
+    gate = jnp.dot(expert_rows, gate_weight[0], preferred_element_type=jnp.float32)
+    up = jnp.dot(expert_rows, up_weight[0], preferred_element_type=jnp.float32)
+    hidden = (jax.nn.silu(gate) * up).astype(jnp.bfloat16)
+    part = jnp.dot(hidden, down_weight[0], preferred_element_type=jnp.float32)
+    part = (part * scale).astype(jnp.bfloat16)
+    mixed_rows, home = collect(
+        part.reshape(GROUPS, 2, tp_count, slots, model_width),
+        proj.reshape(tp_count, sub, model_width),
+    )
+    home = home.reshape(GROUPS * slots, model_width)
+    routed_out = jnp.dot(
+        pick.T.astype(jnp.bfloat16), home, preferred_element_type=jnp.float32
+    ).astype(jnp.bfloat16)
+    return (mixed_rows, routed_out)
 
 
 def shards(
@@ -157,8 +663,9 @@
 
 
 def solution(mesh):
+    paired = mesh.shape["ep"] == 2 * GROUPS and mesh.shape["tp"] == 4
     return jax.shard_map(
-        shards,
+        shards_paired if paired else shards,
         mesh=mesh,
         in_specs=(
             P("ep", "tp"),

time: 290 us -> 139 us (0.48)
  waiting for transfers between devices: 155 us -> 0 us
  Pallas kernels: 0 us -> 107 us
  blocking collectives: 59.1 us -> 0 us
  other arithmetic: 21.6 us -> 4.78 us
  between operations: 15.4 us -> 0.76 us
  local copies, waits for them, and re-layouts: 13 us -> 2.95 us
  starting transfers between devices: 5.71 us -> 0 us
  matrix products: 19 us -> 22.7 us
    pallas_call x0 -> x4, Pallas kernels: none -> 107 us  [the longest x1 43.5 us: collect(): pl.pallas_call(collect_kernel, out_shape=(jax.ShapeDtypeStruct((sub, mode...]
    all_gather x3 -> x0, waiting for transfers between devices: 94.8 us -> none  [the longest x1 57.7 us: shards(): lax.all_gather(value_rows, 'ep', axis=0, tiled=True)]
    reduce_scatter x2 -> x0, waiting for transfers between devices: 60.6 us -> none  [the longest x1 44.3 us: shards(): lax.psum_scatter(jnp.dot(attended, out_weight, preferred_element_type=jnp...]
    all_to_all x1 -> x0, blocking collectives: 32.9 us -> none  [shards(): lax.all_to_all(outgoing, 'ep', split_axis=0, concat_axis=0, tiled=True)]
    all_gather x1 -> x0, blocking collectives: 26.2 us -> none  [shards(): lax.all_gather(key_shift, 'ep', axis=0, tiled=True)]
    another operation x4 -> x1, other arithmetic: 10.5 us -> 0.01 us
    convert_element_type x5 -> x2, other arithmetic: 9.38 us -> 0.68 us  [the longest x1 0.67 us: stick(): tri = (position[:, None] > position[None, :]).astype(jnp.bfloat16)]
    all_to_all x1 -> x0, starting transfers between devices: 5.51 us -> none  [shards(): lax.all_to_all(partial_value.reshape(expert_count, capacity, model_width)...]
  transfers between devices with their start and end apart: 6 -> 0, of which waited for: 5 -> 0; matrix products, arithmetic and copies ran while one was open for 14% -> 0% of each run, Pallas kernels for 0% -> 0%
where the time goes in v1:
time: 139 us; the launch traced here: 138 us
  Pallas kernels  107 us (77%)
  matrix products  22.7 us (16%)
  other arithmetic  4.78 us (3%)
  local copies, waits for them, and re-layouts  2.95 us (2%)
    pallas_call x1, Pallas kernels, collect(): pl.pallas_call(collect_kernel, out_shape=(jax.ShapeDtypeStruct((sub, mode...  43.5 us
    pallas_call x1, Pallas kernels, spread(): pl.pallas_call(kernel, out_shape=(jax.ShapeDtypeStruct((3, block * ep_cou...  43.4 us
    pallas_call x1, Pallas kernels, regroup(): pl.pallas_call(kernel, out_shape=jax.ShapeDtypeStruct((rows // ep_count,...  10.8 us
    dot_general x1, matrix products, shards_paired(): part = jnp.dot(hidden, down_weight[0], preferred_element_type=jnp.float32)  9.54 us
    pallas_call x1, Pallas kernels, stick(): pl.pallas_call(stick_kernel, out_shape=jax.ShapeDtypeStruct(qkv.shape[1:]...  8.91 us
    dot_general x1, matrix products, shards_paired(): jnp.dot(attended, out_weight, preferred_element_type=jnp.float32)  5.65 us
    dot_general x1, matrix products, shards_paired(): jnp.dot(expert_rows, gate_weight[0], preferred_element_type=jnp.float32)  4.12 us

profile of v1, /device:TPU:0, one launch (start us, length us, event | category | flops | bytes accessed | tf_op | source)
XLA Modules:
  0.0 137.8 jit_solution(16356260156026770840)
XLA Ops:
  0.6 0.0 copy-start
  0.7 0.9 and_select_fusion
  1.6 0.7 fusion.35
  2.3 0.2 convert_reduce_fusion
  2.5 0.1 select_reduce_fusion
  2.6 0.1 copy.24
  2.8 1.3 pad_convert_fusion.refs_3_
  4.1 0.7 fusion.30.tri_ref
  4.7 1.4 convolution_convert_fusion.1
  6.1 0.9 fusion.22
  7.0 43.4 %shard_map.122 = (bf16[3,1024,128]{2,1,0:T(8,128)(2,1)}, f32[8,8,128]{2,1,0:T(8,128)}, bf16[4,2,4,16,4224]{4,3,2,1,0:T(8,128)(2,1)}) custom-call(bf16[128,1024]{1,0:T(8,128)(2,1)} %refs_0_.1, bf16[128,1024]{1,0:T(8,128)(2,1)} %refs_1_.1, bf16[128,1024]{1,0:T(8,128)(2,1)} %refs_2_.1, f32[8,8,128]{2,1,0:T(8,128)} %pad_convert_fusion.refs_3_, ...), custom_call_target="tpu_custom_call" | custom-call | tf_op jit(solution)/shard_map/pallas_call | solution.py:242
  50.4 0.9 slice.25
  51.3 0.1 constant_dynamic-slice_fusion
  51.4 0.1 copy.27
  51.6 8.9 %shard_map.123.refs_0_ = bf16[1024,128]{1,0:T(8,128)(2,1)} custom-call(bf16[3,1024,128]{2,1,0:T(8,128)(2,1)} %get-tuple-element.8.qkv_ref, f32[8,8,128]{2,1,0:T(8,128)} %get-tuple-element.9.shift_ref, bf16[256,256]{1,0:T(8,128)(2,1)} %fusion.30.tri_ref), custom_call_target="tpu_custom_call" | custom-call | tf_op jit(solution)/shard_map/pallas_call | solution.py:327
  60.5 10.8 %shard_map.124 = bf16[128,1024]{1,0:T(8,128)(2,1)} custom-call(bf16[1024,128]{1,0:T(8,128)(2,1)} %shard_map.123.refs_0_), custom_call_target="tpu_custom_call" | custom-call | tf_op jit(solution)/shard_map/pallas_call | solution.py:364
  71.3 4.1 %fusion.2 = f32[512,256]{1,0:T(8,128)S(1)} fusion(bf16[512,4224]{1,0:T(8,128)(2,1)} %bitcast.59, bf16[1,4096,256]{2,1,0:T(8,128)(2,1)} %param.19), kind=kOutput, calls=%fused_computation.6 | convolution fusion | flops 1073741824 | bytes 6815744 | tf_op jit(solution)/shard_map/dot_general | solution.py:576
  75.4 0.0 copy-done
  75.4 9.5 %multiply_convert_fusion = bf16[512,4096]{1,0:T(8,128)(2,1)} fusion(f32[512]{0:T(512)S(1)} %bitcast.61, bf16[1,256,4096]{2,1,0:T(8,128)(2,1)S(1)} %copy-done, bf16[1,4096,256]{2,1,0:T(8,128)(2,1)} %param.20, bf16[512,4224]{1,0:T(8,128)(2,1)} %bitcast.60, f32[512,256]{1,0:T(8,128)S(1)} %fusion.2), kind=kOutput, calls=%fused_computation | convolution fusion | flops 2152464384 | bytes 13109248 | tf_op jit(solution)/shard_map/dot_general | solution.py:579
  85.0 0.0 copy-done.1
  85.0 5.6 %convolution_convert_fusion = bf16[128,4096]{1,0:T(8,128)(2,1)} fusion(bf16[128,1024]{1,0:T(8,128)(2,1)S(1)} %copy-done.1, bf16[1024,4096]{1,0:T(8,128)(2,1)} %param.15), kind=kOutput, calls=%fused_computation.1 | convolution fusion | flops 1074266112 | bytes 9699328 | tf_op jit(solution)/shard_map/dot_general | solution.py:570
  90.6 43.5 %shard_map.125 = (bf16[32,4096]{1,0:T(8,128)(2,1)}, bf16[4,16,4096]{2,1,0:T(8,128)(2,1)}) custom-call(bf16[4,2,4,16,4096]{4,3,2,1,0:T(8,128)(2,1)} %bitcast.53, bf16[4,32,4096]{2,1,0:T(8,128)(2,1)} %bitcast.54), custom_call_target="tpu_custom_call" | custom-call | tf_op jit(solution)/shard_map/pallas_call | solution.py:498
  134.1 2.0 %convolution_convert_fusion.2 = bf16[32,4096]{1,0:T(8,128)(2,1)} fusion(bf16[64,4096]{1,0:T(8,128)(2,1)} %bitcast.56, s32[32]{0:T(128)S(1)} %multiply_add_fusion), kind=kOutput, calls=%fused_computation.3 | convolution fusion | flops 16910336 | bytes 786560 | tf_op jit(solution)/shard_map/dot_general | solution.py:586
  136.1 1.7 %copy.29 = bf16[32,4096]{1,0:T(8,128)(2,1)} copy(bf16[32,4096]{1,0:T(8,128)(2,1)} %get-tuple-element.29) | data formatting | bytes 524288
  (8 shorter events, 0.1 us)
Async XLA Ops:
  0.6 74.8 %copy-start = (bf16[1,256,4096]{2,1,0:T(8,128)(2,1)S(1)}, bf16[1,256,4096]{2,1,0:T(8,128)(2,1)}, u32[]{:S(2)}) copy-start(bf16[1,256,4096]{2,1,0:T(8,128)(2,1)} %param.21) | copy-start | bytes 6291460
  75.4 9.6 %copy-start.1 = (bf16[128,1024]{1,0:T(8,128)(2,1)S(1)}, bf16[128,1024]{1,0:T(8,128)(2,1)}, u32[]{:S(2)}) copy-start(bf16[128,1024]{1,0:T(8,128)(2,1)} %shard_map.124) | copy-start | bytes 786436

commit v2 on v0

--- a/solution.py
+++ b/solution.py
@@ -1,10 +1,15 @@
 import jax
 import jax.numpy as jnp
 from jax import lax
+from jax.experimental import pallas as pl
+from jax.experimental.pallas import tpu as pltpu
 from jax.sharding import PartitionSpec as P
 
 HEAD = 64
 KEY_BLOCK = 512
+GROUPS = 4
+TILE = 256
+MESH = pl.DeviceIdType.MESH
 
 
 def stick_attend(query_rows, key_all, value_all, shift_all, first_pos):
@@ -81,6 +86,443 @@
     )
     up_proj = jnp.einsum("rcd,df->rcf", expert_rows, up_part, preferred_element_type=jnp.float32)
     return (jax.nn.silu(gate_proj) * up_proj).astype(jnp.bfloat16)
+
+
+def meet(devices):
+    barrier = pltpu.get_barrier_semaphore()
+    for ep_to, tp_to in devices:
+        pl.semaphore_signal(
+            barrier, inc=1, device_id={"ep": ep_to, "tp": tp_to}, device_id_type=MESH
+        )
+    pl.semaphore_wait(barrier, len(devices))
+
+
+def push(src, dst, send, recv, ep_to, tp_to):
+    copy = pltpu.make_async_remote_copy(
+        src_ref=src,
+        dst_ref=dst,
+        send_sem=send,
+        recv_sem=recv,
+        device_id={"ep": ep_to, "tp": tp_to},
+        device_id_type=MESH,
+    )
+    copy.start()
+    return copy
+
+
+def fused_kernel(
+    ep_count,
+    q_ref, k_ref, v_ref, s_ref, rows_ref, tri_ref, ow_hbm, gw_hbm, uw_hbm, dw_hbm,
+    mixed_ref, home_ref,
+    ow, gw, uw, dw, qkv, shifts, gath, part, got_c, pair, got1, mid, got2, final,
+    att, att_all, proj, got_o, pair_o, got_oy,
+    send_a, recv_a, send_b, recv_b, send_r, recv_r, send_s, recv_s, own_sem, load_sem,
+):
+    e = lax.axis_index("ep")
+    t = lax.axis_index("tp")
+    g = e // 2
+    x = e % 2
+    y = t // 2
+    c = t % 2
+    e_x = g * 2 + (1 - x)
+    t_y = (t + 2) % 4
+    t_c = t + 1 - 2 * c
+    t_yc = (t_c + 2) % 4
+    block = q_ref.shape[0]
+    width = q_ref.shape[1] // ep_count
+    slots = rows_ref.shape[1]
+    model = mixed_ref.shape[1]
+    order = (0, 3, 1, 2)
+    x_first = (0, 1)
+
+    loads = []
+    for n, (src, dst) in enumerate(((gw_hbm, gw), (uw_hbm, uw), (dw_hbm, dw), (ow_hbm, ow))):
+        load = pltpu.make_async_copy(src, dst, load_sem.at[n])
+        load.start()
+        loads.append(load)
+    owns = []
+
+    def keep(src, dst):
+        own = pltpu.make_async_copy(src, dst, own_sem.at[len(owns)])
+        own.start()
+        owns.append(own)
+        return own
+
+    mine = pl.ds(pl.multiple_of(e * width, width), width)
+    here = pl.ds(pl.multiple_of(e * block, block), block)
+    kept_rows = keep(rows_ref.at[g], gath.at[g, x, t])
+    for i, ref in enumerate((q_ref, k_ref, v_ref)):
+        keep(ref.at[:, mine], qkv.at[i, here])
+    keep(s_ref.at[e], shifts.at[e])
+    meet([((e + d) % ep_count, t) for d in range(1, ep_count)] + [(e, t_y), (e, t_c)])
+
+    sends = []
+
+    def send_rows(src, z, xi, ti, ep_to, tp_to):
+        sends.append(
+            push(
+                src, gath.at[z, xi, ti], send_b.at[len(sends)], recv_b.at[z, xi, ti], ep_to, tp_to
+            )
+        )
+
+    def forward(z, xi, ti, ep_to, tp_to):
+        send_rows(gath.at[z, xi, ti], z, xi, ti, ep_to, tp_to)
+
+    def arrived(z, xi, ti):
+        place = gath.at[z, xi, ti]
+        pltpu.make_async_copy(place, place, recv_b.at[z, xi, ti]).wait()
+
+    for dz in (3, 1, 2):
+        to = (g + dz) % GROUPS
+        send_rows(rows_ref.at[to], g, x, t, to * 2 + x, t)
+    for ep_to, tp_to in ((e_x, t), (e, t_y), (e, t_c)):
+        send_rows(rows_ref.at[g], g, x, t, ep_to, tp_to)
+    exchange = []
+    for d in range(1, ep_count):
+        to = (e + d) % ep_count
+        cols = pl.ds(pl.multiple_of(to * width, width), width)
+        for i, ref in enumerate((q_ref, k_ref, v_ref)):
+            exchange.append(
+                push(
+                    ref.at[:, cols], qkv.at[i, here],
+                    send_a.at[i, d - 1], recv_a.at[i, d - 1], to, t,
+                )
+            )
+        exchange.append(
+            push(s_ref.at[to], shifts.at[e], send_a.at[3, d - 1], recv_a.at[3, d - 1], to, t)
+        )
+
+    later_sends = []
+
+    def go(src, dst, ep_to, tp_to):
+        n = len(later_sends)
+        copy = push(src, dst, send_s.at[n], recv_s.at[n], ep_to, tp_to)
+        later_sends.append(copy)
+        return copy
+
+    def add(a, b):
+        return (a.astype(jnp.float32) + b.astype(jnp.float32)).astype(jnp.bfloat16)
+
+    def plane_of(dz):
+        return (g + dz) % GROUPS
+
+    def first_leg(dz):
+        z = plane_of(dz)
+        arrived(z, x, t)
+        forward(z, x, t, e_x, t)
+        forward(z, x, t, e, t_y)
+        forward(z, x, t, e, t_c)
+
+    def second_leg(dz):
+        z = plane_of(dz)
+        arrived(z, 1 - x, t)
+        if dz in (0, 3):
+            forward(z, 1 - x, t, e, t_y)
+        forward(z, 1 - x, t, e, t_c)
+        arrived(z, x, t_y)
+        if dz not in (0, 3):
+            forward(z, x, t_y, e_x, t)
+        forward(z, x, t_y, e, t_c)
+
+    def third_leg(dz):
+        z = plane_of(dz)
+        arrived(z, 1 - x, t_y)
+        forward(z, 1 - x, t_y, e, t_c)
+
+    lane = lax.broadcasted_iota(jnp.int32, (2 * 4 * slots, rows_ref.shape[2] - model), 1)
+    chosen = (lane >= 3 * x) & (lane < 3 * x + 3)
+    swaps = {}
+    hops = {}
+    ends = {}
+
+    def experts(dz):
+        z = plane_of(dz)
+        for xi in (x, 1 - x):
+            arrived(z, xi, t_c)
+            arrived(z, xi, t_yc)
+        rows = gath[z].reshape(2 * 4 * slots, rows_ref.shape[2])
+        inputs = rows[:, :model]
+        marks = rows[:, model:].astype(jnp.float32)
+        scale = jnp.sum(jnp.where(chosen, marks, 0.0), axis=1, keepdims=True)
+        gate = jnp.dot(inputs, gw[...], preferred_element_type=jnp.float32)
+        up = jnp.dot(inputs, uw[...], preferred_element_type=jnp.float32)
+        hidden = (gate / (1.0 + jnp.exp(-gate)) * up).astype(jnp.bfloat16)
+        step = model // 4
+        for n in range(4):
+            cols = slice(n * step, (n + 1) * step)
+            down = jnp.dot(hidden, dw[:, cols], preferred_element_type=jnp.float32)
+            down = (down * scale).astype(jnp.bfloat16)
+            for xi in range(2):
+                for ti in range(4):
+                    at = (xi * 4 + ti) * slots
+                    part[dz, ti % 2, xi, ti // 2, :, cols] = down[at : at + slots]
+        swaps[dz] = go(part.at[dz, 1 - c], got_c.at[dz], e, t_c)
+
+    def pair_sum(dz):
+        swaps[dz].wait_recv()
+        pair[dz] = add(part[dz, c], got_c[dz])
+        if dz in x_first:
+            hops[dz] = go(pair.at[dz, 1 - x], got1.at[dz], e_x, t)
+        else:
+            hops[dz] = go(pair.at[dz, :, 1 - y], got1.at[dz], e, t_y)
+
+    def middle_sum(dz):
+        hops[dz].wait_recv()
+        if dz in x_first:
+            mid[dz] = add(pair[dz, x], got1[dz])
+            ends[dz] = go(mid.at[dz, 1 - y], got2.at[dz], e, t_y)
+        else:
+            mid[dz] = add(pair[dz, :, y], got1[dz])
+            ends[dz] = go(mid.at[dz, 1 - x], got2.at[dz], e_x, t)
+
+    backs = []
+
+    def send_home(dz):
+        ends[dz].wait_recv()
+        total = add(mid[dz, y if dz in x_first else x], got2[dz])
+        if dz == 0:
+            home_ref[g] = total
+        else:
+            final[dz] = total
+            backs.append(go(final.at[dz], home_ref.at[g], plane_of(dz) * 2 + x, t))
+
+    kept_rows.wait()
+    second_leg(0)
+    first_leg(3)
+    first_leg(1)
+    second_leg(3)
+    third_leg(0)
+    first_leg(2)
+    second_leg(1)
+    third_leg(3)
+    for load in loads[:3]:
+        load.wait()
+    experts(0)
+    second_leg(2)
+    third_leg(1)
+    experts(3)
+    third_leg(2)
+    pair_sum(0)
+    experts(1)
+    pair_sum(3)
+    experts(2)
+    pair_sum(1)
+    pair_sum(2)
+    for copy in exchange:
+        copy.wait()
+    for own in owns[1:]:
+        own.wait()
+    tri = tri_ref[...]
+    middle_sum(0)
+    middle_sum(3)
+    blocks = att.shape[0] // TILE
+    stick_block(blocks - 1, qkv, shifts, tri, att)
+    middle_sum(1)
+    middle_sum(2)
+    for i in range(blocks - 2, -1, -1):
+        stick_block(i, qkv, shifts, tri, att)
+    regroups = []
+    for d in range(1, ep_count):
+        to = (e + d) % ep_count
+        rows = pl.ds(pl.multiple_of(to * block, block), block)
+        regroups.append(
+            push(
+                att.at[rows], att_all.at[:, mine], send_r.at[d - 1], recv_r.at[d - 1], to, t
+            )
+        )
+    own_heads = keep(att.at[here], att_all.at[:, mine])
+    for dz in (3, 1, 2, 0):
+        send_home(dz)
+    for copy in regroups:
+        copy.wait()
+    own_heads.wait()
+    loads[3].wait()
+    sub = mixed_ref.shape[0]
+    chunk = 512
+
+    def project(n, carry):
+        cols = pl.ds(pl.multiple_of(n * chunk, chunk), chunk)
+        value = jnp.dot(att_all[...], ow[:, cols], preferred_element_type=jnp.float32)
+        value = value.astype(jnp.bfloat16)
+        for ti in range(4):
+            proj[ti % 2, ti // 2, :, cols] = value[ti * sub : (ti + 1) * sub]
+        return carry
+
+    lax.fori_loop(0, model // chunk, project, 0)
+    swap_o = go(proj.at[1 - c], got_o, e, t_c)
+    swap_o.wait_recv()
+    pair_o[1 - y] = add(proj[c, 1 - y], got_o[1 - y])
+    hop_o = go(pair_o.at[1 - y], got_oy, e, t_y)
+    pair_o[y] = add(proj[c, y], got_o[y])
+    hop_o.wait_recv()
+    mixed_ref[...] = add(pair_o[y], got_oy[...])
+    for copy in backs:
+        copy.wait_recv()
+    for copy in sends + later_sends:
+        copy.wait_send()
+
+
+def stick_block(i, qkv, shifts, tri, out_ref):
+    width = qkv.shape[2]
+    heads = width // HEAD
+    per = shifts.shape[2]
+    score_scale = HEAD ** (-0.5)
+    lane = lax.broadcasted_iota(jnp.int32, (TILE, width), 1) // HEAD
+    strict = lax.broadcasted_iota(jnp.int32, (TILE, TILE), 1) < lax.broadcasted_iota(
+        jnp.int32, (TILE, TILE), 0
+    )
+    q_all = qkv[0, i * TILE : (i + 1) * TILE]
+    q_heads = [jnp.where(lane == h, q_all, jnp.zeros_like(q_all)) for h in range(heads)]
+    running = [jnp.zeros((TILE, width), jnp.float32) for _ in range(heads)]
+    logsum = [jnp.zeros((TILE, 1), jnp.float32) for _ in range(heads)]
+    for j in range(i, -1, -1):
+        k_all = qkv[1, j * TILE : (j + 1) * TILE]
+        v_all = qkv[2, j * TILE : (j + 1) * TILE]
+        for h in range(heads):
+            shift = jnp.concatenate(
+                [shifts[j * (TILE // per) + p, h : h + 1] for p in range(TILE // per)], axis=1
+            )
+            score = (
+                lax.dot_general(
+                    q_heads[h],
+                    k_all,
+                    (((1,), (1,)), ((), ())),
+                    preferred_element_type=jnp.float32,
+                )
+                * score_scale
+                + shift
+            )
+            tail = jnp.log(1.0 + jnp.exp(-jnp.abs(score)))
+            log_take = jnp.minimum(score, 0.0) - tail
+            log_keep = -jnp.maximum(score, 0.0) - tail
+            if i == j:
+                log_keep = jnp.where(strict, log_keep, 0.0)
+            high = log_keep.astype(jnp.bfloat16)
+            low = (log_keep - high.astype(jnp.float32)).astype(jnp.bfloat16)
+            later = jnp.dot(high, tri, preferred_element_type=jnp.float32) + jnp.dot(
+                low, tri, preferred_element_type=jnp.float32
+            )
+            weight = jnp.exp(log_take + later + logsum[h])
+            if i == j:
+                weight = jnp.where(strict, weight, 0.0)
+            running[h] = running[h] + jnp.dot(
+                weight.astype(jnp.bfloat16), v_all, preferred_element_type=jnp.float32
+            )
+            logsum[h] = logsum[h] + later[:, :1] + log_keep[:, :1]
+    result = running[0]
+    for h in range(1, heads):
+        result = jnp.where(lane == h, running[h], result)
+    out_ref[i * TILE : (i + 1) * TILE] = result.astype(jnp.bfloat16)
+
+
+def fused(q, k, v, shift_rows, rows, out_w, gate_w, up_w, down_w, ep_count, tp_count):
+    block = q.shape[0]
+    width = q.shape[1] // ep_count
+    slots, row_width = rows.shape[1:]
+    model = out_w.shape[1]
+    sub = block // tp_count
+    position = jnp.arange(TILE, dtype=jnp.int32)
+    tri = (position[:, None] > position[None, :]).astype(jnp.bfloat16)
+    vmem_spec = pl.BlockSpec(memory_space=pltpu.VMEM)
+    any_spec = pl.BlockSpec(memory_space=pl.ANY)
+    bf = jnp.bfloat16
+    dma = pltpu.SemaphoreType.DMA
+    one = (slots, model)
+
+    def kernel(*refs):
+        fused_kernel(ep_count, *refs)
+
+    return pl.pallas_call(
+        kernel,
+        out_shape=(
+            jax.ShapeDtypeStruct((sub, model), bf),
+            jax.ShapeDtypeStruct((GROUPS, *one), bf),
+        ),
+        in_specs=[vmem_spec] * 6 + [any_spec] * 4,
+        out_specs=(vmem_spec,) * 2,
+        scratch_shapes=[
+            pltpu.VMEM(out_w.shape, bf),
+            pltpu.VMEM(gate_w.shape, bf),
+            pltpu.VMEM(up_w.shape, bf),
+            pltpu.VMEM(down_w.shape, bf),
+            pltpu.VMEM((3, block * ep_count, width), bf),
+            pltpu.VMEM(shift_rows.shape, jnp.float32),
+            pltpu.VMEM((GROUPS, 2, tp_count, slots, row_width), bf),
+            pltpu.VMEM((GROUPS, 2, 2, 2, *one), bf),
+            pltpu.VMEM((GROUPS, 2, 2, *one), bf),
+            pltpu.VMEM((GROUPS, 2, 2, *one), bf),
+            pltpu.VMEM((GROUPS, 2, *one), bf),
+            pltpu.VMEM((GROUPS, 2, *one), bf),
+            pltpu.VMEM((GROUPS, *one), bf),
+            pltpu.VMEM((GROUPS, *one), bf),
+            pltpu.VMEM((block * ep_count, width), bf),
+            pltpu.VMEM(q.shape, bf),
+            pltpu.VMEM((2, 2, sub, model), bf),
+            pltpu.VMEM((2, sub, model), bf),
+            pltpu.VMEM((2, sub, model), bf),
+            pltpu.VMEM((sub, model), bf),
+            dma((4, ep_count - 1)),
+            dma((4, ep_count - 1)),
+            dma((31,)),
+            dma((GROUPS, 2, tp_count)),
+            dma((ep_count - 1,)),
+            dma((ep_count - 1,)),
+            dma((17,)),
+            dma((17,)),
+            dma((6,)),
+            dma((4,)),
+        ],
+        compiler_params=pltpu.CompilerParams(
+            collective_id=0, has_side_effects=True, vmem_limit_bytes=60000 * 1024
+        ),
+    )(q, k, v, shift_rows, rows, tri, out_w, gate_w, up_w, down_w)
+
+
+def shards_paired(
+    queries, key_rows, value_rows, key_shift, out_weight, routed_rows, expert_ids,
+    route_weights, gate_weight, up_weight, down_weight,
+):
+    ep_count = lax.axis_size("ep")
+    tp_count = lax.axis_size("tp")
+    local_rows = queries.shape[0]
+    sub = local_rows // tp_count
+    slots = 4 * sub // ep_count
+    model_width = routed_rows.shape[1]
+    column = lax.axis_index("tp")
+
+    ids = lax.dynamic_slice_in_dim(expert_ids, column * sub, sub, 0)
+    own_rows = lax.dynamic_slice_in_dim(routed_rows, column * sub, sub, 0)
+    group = ids[:, 0] // 2
+    token = jnp.arange(sub, dtype=jnp.int32)
+    earlier = (group[:, None] == group[None, :]) & (token[None, :] < token[:, None])
+    place = group * slots + jnp.sum(earlier.astype(jnp.int32), axis=1)
+    pick = place[None, :] == jnp.arange(GROUPS * slots, dtype=jnp.int32)[:, None]
+    packed = jnp.dot(pick.astype(jnp.bfloat16), own_rows, preferred_element_type=jnp.float32)
+    side = [
+        jnp.sum(jnp.where(ids % 2 == s, route_weights, 0.0), axis=1) for s in range(2)
+    ]
+    pieces = []
+    for weights in side:
+        spread_w = jnp.sum(jnp.where(pick, weights[None, :], 0.0), axis=1)
+        first = lax.reduce_precision(spread_w, 8, 7)
+        second = lax.reduce_precision(spread_w - first, 8, 7)
+        pieces += [first, second, spread_w - first - second]
+    extra = jnp.pad(jnp.stack(pieces, axis=1), ((0, 0), (0, 128 - len(pieces))))
+    rows = jnp.concatenate([packed.astype(jnp.bfloat16), extra.astype(jnp.bfloat16)], axis=1)
+    rows = rows.reshape(GROUPS, slots, model_width + 128)
+
+    per = key_shift.shape[1] // ep_count
+    shift_rows = key_shift.astype(jnp.float32).T.reshape(ep_count, per, local_rows)
+    shift_rows = jnp.pad(shift_rows, ((0, 0), (0, -per % 8), (0, 0)))
+    mixed_rows, home = fused(
+        queries, key_rows, value_rows, shift_rows, rows,
+        out_weight, gate_weight[0], up_weight[0], down_weight[0], ep_count, tp_count,
+    )
+    home = home.reshape(GROUPS * slots, model_width)
+    routed_out = jnp.dot(
+        pick.T.astype(jnp.bfloat16), home, preferred_element_type=jnp.float32
+    ).astype(jnp.bfloat16)
+    return (mixed_rows, routed_out)
 
 
 def shards(
@@ -157,8 +599,9 @@
 
 
 def solution(mesh):
+    paired = mesh.shape["ep"] == 2 * GROUPS and mesh.shape["tp"] == 4
     return jax.shard_map(
-        shards,
+        shards_paired if paired else shards,
         mesh=mesh,
         in_specs=(
             P("ep", "tp"),

time: 290 us -> 90.6 us (0.31)
  the two profiles are of different devices: /device:TPU:0 before, /device:TPU:31 now
where the time goes in v2:
time: 90.6 us; the launch traced here: 90.3 us
  Pallas kernels  80.7 us (89%)
  other arithmetic  4.67 us (5%)
  matrix products  2.43 us (3%)
  local copies, waits for them, and re-layouts  1.83 us (2%)
    pallas_call x1, Pallas kernels, fused(): pl.pallas_call(kernel, out_shape=(jax.ShapeDtypeStruct((sub, model), bf),...  80.7 us
    dot_general x1, matrix products, shards_paired(): jnp.dot(pick.T.astype(jnp.bfloat16), home, preferred_element_type=jnp.flo...  2.02 us

profile of v2, /device:TPU:31, one launch (start us, length us, event | category | flops | bytes accessed | tf_op | source)
XLA Modules:
  0.0 90.3 jit_solution(9854869041444087484)
XLA Ops:
  0.6 0.0 copy-start
  0.6 0.8 and_select_fusion
  1.5 0.7 fusion.8
  2.2 0.2 convert_reduce_fusion
  2.4 0.1 select_reduce_fusion
  2.6 0.1 copy.18
  2.7 1.3 %pad_convert_fusion.refs_3_ = f32[8,8,128]{2,1,0:T(8,128)} fusion(bf16[8,2,128]{2,1,0:T(2,128)(2,1)} %bitcast.40), kind=kLoop, calls=%fused_computation.13 | loop fusion | flops 8192 | bytes 36864 | tf_op jit(solution)/shard_map/jit(_pad)/pad | solution.py:516
  4.0 0.7 fusion.3.refs_5_
  4.7 0.0 copy-done
  4.7 0.4 convolution_convert_fusion
  5.1 0.8 fusion.1
  5.9 80.7 %shard_map.122 = (bf16[32,4096]{1,0:T(8,128)(2,1)}, bf16[4,16,4096]{2,1,0:T(8,128)(2,1)}) custom-call(bf16[128,1024]{1,0:T(8,128)(2,1)} %refs_0_.1, bf16[128,1024]{1,0:T(8,128)(2,1)} %refs_1_.1, bf16[128,1024]{1,0:T(8,128)(2,1)} %refs_2_.1, f32[8,8,128]{2,1,0:T(8,128)} %pad_convert_fusion.refs_3_, bf16[4,16,4224]{2,1,0:T(8,128)(2,1)} %bitcast.35, ...), custom_call_target="tpu_custom_call" | custom-call | tf_op jit(solution)/shard_map/pallas_call | solution.py:435
  86.6 2.0 %convolution_convert_fusion.1 = bf16[32,4096]{1,0:T(8,128)(2,1)} fusion(bf16[64,4096]{1,0:T(8,128)(2,1)} %bitcast.39, s32[32]{0:T(128)S(1)} %multiply_add_fusion), kind=kOutput, calls=%fused_computation.1 | convolution fusion | flops 16910336 | bytes 786560 | tf_op jit(solution)/shard_map/dot_general | solution.py:522
  88.7 1.7 %copy.20 = bf16[32,4096]{1,0:T(8,128)(2,1)} copy(bf16[32,4096]{1,0:T(8,128)(2,1)} %get-tuple-element.23) | data formatting | bytes 524288
  (5 shorter events, 0.1 us)
Async XLA Ops:
  0.6 4.0 %copy-start = (bf16[128,4096]{1,0:T(8,128)(2,1)S(1)}, bf16[128,4096]{1,0:T(8,128)(2,1)}, u32[]{:S(2)}) copy-start(bf16[128,4096]{1,0:T(8,128)(2,1)} %param.16) | copy-start | bytes 3145732

commit v3 on v2

--- a/solution.py
+++ b/solution.py
@@ -112,7 +112,7 @@
 
 def fused_kernel(
     ep_count,
-    q_ref, k_ref, v_ref, s_ref, rows_ref, tri_ref, ow_hbm, gw_hbm, uw_hbm, dw_hbm,
+    q_ref, k_ref, v_ref, s_ref, rows_ref, ow_hbm, gw_hbm, uw_hbm, dw_hbm,
     mixed_ref, home_ref,
     ow, gw, uw, dw, qkv, shifts, gath, part, got_c, pair, got1, mid, got2, final,
     att, att_all, proj, got_o, pair_o, got_oy,
@@ -178,19 +178,23 @@
     for ep_to, tp_to in ((e_x, t), (e, t_y), (e, t_c)):
         send_rows(rows_ref.at[g], g, x, t, ep_to, tp_to)
     exchange = []
-    for d in range(1, ep_count):
-        to = (e + d) % ep_count
-        cols = pl.ds(pl.multiple_of(to * width, width), width)
-        for i, ref in enumerate((q_ref, k_ref, v_ref)):
+
+    def exchange_heads(distances):
+        for d in distances:
+            to = (e + d) % ep_count
+            cols = pl.ds(pl.multiple_of(to * width, width), width)
+            for i, ref in enumerate((q_ref, k_ref, v_ref)):
+                exchange.append(
+                    push(
+                        ref.at[:, cols], qkv.at[i, here],
+                        send_a.at[i, d - 1], recv_a.at[i, d - 1], to, t,
+                    )
+                )
             exchange.append(
-                push(
-                    ref.at[:, cols], qkv.at[i, here],
-                    send_a.at[i, d - 1], recv_a.at[i, d - 1], to, t,
-                )
-            )
-        exchange.append(
-            push(s_ref.at[to], shifts.at[e], send_a.at[3, d - 1], recv_a.at[3, d - 1], to, t)
-        )
+                push(s_ref.at[to], shifts.at[e], send_a.at[3, d - 1], recv_a.at[3, d - 1], to, t)
+            )
+
+    exchange_heads(range(2, ep_count, 2))
 
     later_sends = []
 
@@ -299,6 +303,7 @@
         load.wait()
     experts(0)
     second_leg(2)
+    exchange_heads(range(1, ep_count, 2))
     third_leg(1)
     experts(3)
     third_leg(2)
@@ -312,15 +317,14 @@
         copy.wait()
     for own in owns[1:]:
         own.wait()
-    tri = tri_ref[...]
+    blocks = att.shape[0] // TILE
+    half = blocks // 2
+    for i in range(blocks - 1, half - 1, -1):
+        stick_block(i, qkv, shifts, att)
     middle_sum(0)
     middle_sum(3)
-    blocks = att.shape[0] // TILE
-    stick_block(blocks - 1, qkv, shifts, tri, att)
-    middle_sum(1)
-    middle_sum(2)
-    for i in range(blocks - 2, -1, -1):
-        stick_block(i, qkv, shifts, tri, att)
+    for i in range(half - 1, -1, -1):
+        stick_block(i, qkv, shifts, att)
     regroups = []
     for d in range(1, ep_count):
         to = (e + d) % ep_count
@@ -331,6 +335,8 @@
             )
         )
     own_heads = keep(att.at[here], att_all.at[:, mine])
+    middle_sum(1)
+    middle_sum(2)
     for dz in (3, 1, 2, 0):
         send_home(dz)
     for copy in regroups:
@@ -362,7 +368,7 @@
         copy.wait_send()
 
 
-def stick_block(i, qkv, shifts, tri, out_ref):
+def stick_block(i, qkv, shifts, out_ref):
     width = qkv.shape[2]
     heads = width // HEAD
     per = shifts.shape[2]
@@ -371,6 +377,12 @@
     strict = lax.broadcasted_iota(jnp.int32, (TILE, TILE), 1) < lax.broadcasted_iota(
         jnp.int32, (TILE, TILE), 0
     )
+    tri = jnp.where(
+        lax.broadcasted_iota(jnp.int32, (TILE, TILE), 0)
+        > lax.broadcasted_iota(jnp.int32, (TILE, TILE), 1),
+        1.0,
+        0.0,
+    ).astype(jnp.bfloat16)
     q_all = qkv[0, i * TILE : (i + 1) * TILE]
     q_heads = [jnp.where(lane == h, q_all, jnp.zeros_like(q_all)) for h in range(heads)]
     running = [jnp.zeros((TILE, width), jnp.float32) for _ in range(heads)]
@@ -421,8 +433,6 @@
     slots, row_width = rows.shape[1:]
     model = out_w.shape[1]
     sub = block // tp_count
-    position = jnp.arange(TILE, dtype=jnp.int32)
-    tri = (position[:, None] > position[None, :]).astype(jnp.bfloat16)
     vmem_spec = pl.BlockSpec(memory_space=pltpu.VMEM)
     any_spec = pl.BlockSpec(memory_space=pl.ANY)
     bf = jnp.bfloat16
@@ -438,7 +448,7 @@
             jax.ShapeDtypeStruct((sub, model), bf),
             jax.ShapeDtypeStruct((GROUPS, *one), bf),
         ),
-        in_specs=[vmem_spec] * 6 + [any_spec] * 4,
+        in_specs=[vmem_spec] * 5 + [any_spec] * 4,
         out_specs=(vmem_spec,) * 2,
         scratch_shapes=[
             pltpu.VMEM(out_w.shape, bf),
@@ -475,7 +485,7 @@
         compiler_params=pltpu.CompilerParams(
             collective_id=0, has_side_effects=True, vmem_limit_bytes=60000 * 1024
         ),
-    )(q, k, v, shift_rows, rows, tri, out_w, gate_w, up_w, down_w)
+    )(q, k, v, shift_rows, rows, out_w, gate_w, up_w, down_w)
 
 
 def shards_paired(

time: 90.6 us -> 85.6 us (0.945)
  the two profiles are of different devices: /device:TPU:31 before, /device:TPU:0 now
where the time goes in v3:
time: 85.6 us; the launch traced here: 85.3 us
  Pallas kernels  76.3 us (89%)
  other arithmetic  4 us (5%)
  matrix products  2.43 us (3%)
  local copies, waits for them, and re-layouts  1.83 us (2%)
    pallas_call x1, Pallas kernels, fused(): pl.pallas_call(kernel, out_shape=(jax.ShapeDtypeStruct((sub, model), bf),...  76.3 us
    dot_general x1, matrix products, shards_paired(): jnp.dot(pick.T.astype(jnp.bfloat16), home, preferred_element_type=jnp.flo...  2.02 us

profile of v3, /device:TPU:0, one launch (start us, length us, event | category | flops | bytes accessed | tf_op | source)
XLA Modules:
  0.0 85.3 jit_solution(3173360503613486275)
XLA Ops:
  0.6 0.0 copy-start
  0.6 0.8 and_select_fusion
  1.5 0.7 fusion.7
  2.2 0.2 convert_reduce_fusion
  2.4 0.1 select_reduce_fusion
  2.6 0.1 copy.18
  2.7 1.3 %pad_convert_fusion.refs_3_ = f32[8,8,128]{2,1,0:T(8,128)} fusion(bf16[8,2,128]{2,1,0:T(2,128)(2,1)} %bitcast.40), kind=kLoop, calls=%fused_computation.11 | loop fusion | flops 8192 | bytes 36864 | tf_op jit(solution)/shard_map/jit(_pad)/pad | solution.py:526
  4.0 0.0 copy-done
  4.0 0.4 convolution_convert_fusion
  4.4 0.8 fusion.1
  5.2 76.3 %shard_map.122 = (bf16[32,4096]{1,0:T(8,128)(2,1)}, bf16[4,16,4096]{2,1,0:T(8,128)(2,1)}) custom-call(bf16[128,1024]{1,0:T(8,128)(2,1)} %refs_0_.1, bf16[128,1024]{1,0:T(8,128)(2,1)} %refs_1_.1, bf16[128,1024]{1,0:T(8,128)(2,1)} %refs_2_.1, f32[8,8,128]{2,1,0:T(8,128)} %pad_convert_fusion.refs_3_, bf16[4,16,4224]{2,1,0:T(8,128)(2,1)} %bitcast.35, ...), custom_call_target="tpu_custom_call" | custom-call | tf_op jit(solution)/shard_map/pallas_call | solution.py:445
  81.6 2.0 %convolution_convert_fusion.1 = bf16[32,4096]{1,0:T(8,128)(2,1)} fusion(bf16[64,4096]{1,0:T(8,128)(2,1)} %bitcast.39, s32[32]{0:T(128)S(1)} %multiply_add_fusion), kind=kOutput, calls=%fused_computation.1 | convolution fusion | flops 16910336 | bytes 786560 | tf_op jit(solution)/shard_map/dot_general | solution.py:532
  83.6 1.7 %copy.20 = bf16[32,4096]{1,0:T(8,128)(2,1)} copy(bf16[32,4096]{1,0:T(8,128)(2,1)} %get-tuple-element.23) | data formatting | bytes 524288
  (5 shorter events, 0.1 us)
Async XLA Ops:
  0.6 3.4 %copy-start = (bf16[128,4096]{1,0:T(8,128)(2,1)S(1)}, bf16[128,4096]{1,0:T(8,128)(2,1)}, u32[]{:S(2)}) copy-start(bf16[128,4096]{1,0:T(8,128)(2,1)} %param.16) | copy-start | bytes 3145732
